TPU v7x, 32 devices: a whole 2x2x4 slice. The times are simulated.
32 devices in a mesh: kv: 8 (over z, x), tp: 4 (over y, core).
Axes of the slice: x: 2, y: 2, z: 4, core: 2. Of those that a mesh axis runs over, the one named last changes fastest.
Arguments:
- layer_input: bfloat16 [256, 4096], P('tp', 'kv'), may hold values from -6 to 6
- seq_lengths: int32 [64], P('kv'), may hold values from 1 to 4, 112 in all
- delta_state: float32 [64, 16, 128, 128], P('kv', 'tp'), may hold values from -0.4 to 0.4
- attn_gain: bfloat16 [4096], replicated, may hold values from 0.099609375 to 1.8984375
- w_query: bfloat16 [4096, 2048], P('kv', 'tp'), may hold values from -0.09375 to 0.09375
- w_key: bfloat16 [4096, 2048], P('kv', 'tp'), may hold values from -0.09375 to 0.09375
- w_value: bfloat16 [4096, 2048], P('kv', 'tp'), may hold values from -0.09375 to 0.09375
- w_outgate: bfloat16 [4096, 2048], P('kv', 'tp'), may hold values from -0.09375 to 0.09375
- w_write: bfloat16 [4096, 16], P('kv', 'tp'), may hold values from -0.09375 to 0.09375
- w_forget: bfloat16 [4096, 16], P('kv', 'tp'), may hold values from -0.09375 to 0.09375
- forget_rate: float32 [16], P('tp'), may hold values from 0.02 to 2
- head_gain: float32 [128], replicated, may hold values from 0.1 to 1.9
- w_out: bfloat16 [2048, 4096], P('tp', 'kv'), may hold values from -0.125 to 0.125
- mixer_gain: bfloat16 [4096], replicated, may hold values from 0.099609375 to 1.8984375
- w_gate: bfloat16 [4096, 11264], P('kv', 'tp'), may hold values from -0.09375 to 0.09375
- w_up: bfloat16 [4096, 11264], P('kv', 'tp'), may hold values from -0.09375 to 0.09375
- w_down: bfloat16 [11264, 4096], P('tp', 'kv'), may hold values from -0.0546875 to 0.0546875
Outputs:
- layer_output: bfloat16 [256, 4096], P('tp', 'kv')
- next_state: float32 [64, 16, 128, 128], P('kv', 'tp')
Inputs may be any that keep to these rules, and one draw needn't show every extreme that they name: `seq_lengths`: the lengths add up to 112.
All inputs are finite; a program needn't handle non-finite values. No bound on the sum of `seq_lengths` on one device may be relied on, other than what follows from the above.
Results may differ from a plain program's by a relative error of at most 0.024.
Values may be sent and summed in bfloat16 or wider, within the bound.
A program may use at most 64 MiB of HBM per device.

v0:
```python
import jax
import jax.numpy as jnp
from jax import lax
from jax.sharding import PartitionSpec as P

D = 4096
NEW = 4


EPS = 1e-06


def unit_norm(vectors):
    return vectors * lax.rsqrt(jnp.sum(vectors * vectors, axis=-1, keepdims=True) + EPS)


def run_delta(carried, query_unit, key_unit, value_act, write_rate, log_keep, live):
    readings = []
    for position in range(query_unit.shape[1]):
        active = live[:, position][:, None]
        beta = write_rate[:, position] * active
        keep = jnp.exp(log_keep[:, position] * active)
        key_now = key_unit[:, position]
        recalled = jnp.einsum("shk,shkv->shv", key_now, carried, precision=lax.Precision.HIGHEST)
        update = beta[:, :, None] * (value_act[:, position] - keep[:, :, None] * recalled)
        carried = keep[:, :, None, None] * carried + key_now[:, :, :, None] * update[:, :, None, :]
        reading = jnp.einsum(
            "shk,shkv->shv", query_unit[:, position], carried, precision=lax.Precision.HIGHEST
        )
        readings.append(reading * active[:, :, None])
    return (carried, jnp.stack(readings, axis=1))


def local(
    layer_input,
    seq_lengths,
    delta_state,
    attn_gain,
    w_query,
    w_key,
    w_value,
    w_outgate,
    w_write,
    w_forget,
    forget_rate,
    head_gain,
    w_out,
    mixer_gain,
    w_gate,
    w_up,
    w_down,
):
    feature_part = layer_input.shape[1]
    feature_anchor = lax.axis_index("kv") * feature_part
    gathered = lax.all_gather(layer_input, "tp", axis=0, tiled=True)
    rows_wide = gathered.astype(jnp.float32)
    squares = jnp.sum(rows_wide * rows_wide, axis=1)
    gain_part = lax.dynamic_slice_in_dim(attn_gain, feature_anchor, feature_part).astype(
        jnp.float32
    )
    normed_in = (rows_wide * gain_part).astype(jnp.bfloat16)
    query_part = jnp.dot(normed_in, w_query, preferred_element_type=jnp.float32)
    key_part = jnp.dot(normed_in, w_key, preferred_element_type=jnp.float32)
    value_part = jnp.dot(normed_in, w_value, preferred_element_type=jnp.float32)
    gate_part = jnp.dot(normed_in, w_outgate, preferred_element_type=jnp.float32)
    rate_part = jnp.dot(
        normed_in, jnp.concatenate([w_write, w_forget], axis=1), preferred_element_type=jnp.float32
    )
    own_rows = gathered.shape[0] // lax.axis_size("kv")
    query_sum, key_sum, value_sum, gate_sum, rate_sum, own_squares = (
        lax.psum_scatter(
            query_part.astype(jnp.bfloat16), "kv", scatter_dimension=0, tiled=True
        ).astype(jnp.float32),
        lax.psum_scatter(
            key_part.astype(jnp.bfloat16), "kv", scatter_dimension=0, tiled=True
        ).astype(jnp.float32),
        lax.psum_scatter(
            value_part.astype(jnp.bfloat16), "kv", scatter_dimension=0, tiled=True
        ).astype(jnp.float32),
        lax.psum_scatter(
            gate_part.astype(jnp.bfloat16), "kv", scatter_dimension=0, tiled=True
        ).astype(jnp.float32),
        lax.psum_scatter(
            rate_part.astype(jnp.bfloat16), "kv", scatter_dimension=0, tiled=True
        ).astype(jnp.float32),
        lax.psum_scatter(
            squares.astype(jnp.bfloat16), "kv", scatter_dimension=0, tiled=True
        ).astype(jnp.float32),
    )
    row_scale = lax.rsqrt(own_squares / D + EPS)[:, None]
    seqs_here = seq_lengths.shape[0]
    heads_here = forget_rate.shape[0]
    head_size = head_gain.shape[0]

    def split_heads(block):
        return (block * row_scale).reshape(seqs_here, NEW, heads_here, head_size)

    query_unit = unit_norm(jax.nn.silu(split_heads(query_sum))) * head_size ** (-0.5)
    key_unit = unit_norm(jax.nn.silu(split_heads(key_sum)))
    value_act = jax.nn.silu(split_heads(value_sum))
    outgate = split_heads(gate_sum)
    rate_rows = (rate_sum * row_scale).reshape(seqs_here, NEW, 2 * heads_here)
    write_rate = jax.nn.sigmoid(rate_rows[:, :, :heads_here])
    log_keep = -forget_rate * jax.nn.softplus(rate_rows[:, :, heads_here:])
    positions = jnp.arange(NEW, dtype=jnp.int32)
    live = (positions[None, :] < seq_lengths[:, None]).astype(jnp.float32)
    carried, readings = run_delta(
        delta_state, query_unit, key_unit, value_act, write_rate, log_keep, live
    )
    normed = readings * lax.rsqrt(jnp.mean(readings * readings, axis=-1, keepdims=True) + EPS)
    normed = normed * head_gain * jax.nn.silu(outgate)
    mixed = normed.reshape(own_rows, heads_here * head_size).astype(jnp.bfloat16)
    out_terms = jnp.dot(
        lax.all_gather(mixed, "kv", axis=0, tiled=True), w_out, preferred_element_type=jnp.float32
    )
    attended = lax.psum_scatter(
        out_terms.astype(jnp.bfloat16), "tp", scatter_dimension=0, tiled=True
    ).astype(jnp.float32)
    hidden_state = (layer_input.astype(jnp.float32) + attended).astype(jnp.bfloat16)
    hidden_rows = lax.all_gather(hidden_state, "tp", axis=0, tiled=True)
    hidden_wide = hidden_rows.astype(jnp.float32)
    mixer_squares = jnp.sum(hidden_wide * hidden_wide, axis=1)
    mixer_part = lax.dynamic_slice_in_dim(mixer_gain, feature_anchor, feature_part).astype(
        jnp.float32
    )
    normed_mid = (hidden_wide * mixer_part).astype(jnp.bfloat16)
    gate_terms = jnp.dot(normed_mid, w_gate, preferred_element_type=jnp.float32)
    up_terms = jnp.dot(normed_mid, w_up, preferred_element_type=jnp.float32)
    gate_rows, up_rows, square_rows = (
        lax.psum_scatter(
            gate_terms.astype(jnp.bfloat16), "kv", scatter_dimension=0, tiled=True
        ).astype(jnp.float32),
        lax.psum_scatter(
            up_terms.astype(jnp.bfloat16), "kv", scatter_dimension=0, tiled=True
        ).astype(jnp.float32),
        lax.psum_scatter(
            mixer_squares.astype(jnp.bfloat16), "kv", scatter_dimension=0, tiled=True
        ).astype(jnp.float32),
    )
    mixer_scale = lax.rsqrt(square_rows / D + EPS)[:, None]
    activated = (jax.nn.silu(mixer_scale * gate_rows) * (mixer_scale * up_rows)).astype(
        jnp.bfloat16
    )
    mixer_terms = jnp.dot(
        lax.all_gather(activated, "kv", axis=0, tiled=True),
        w_down,
        preferred_element_type=jnp.float32,
    )
    mixer_out = lax.psum_scatter(
        mixer_terms.astype(jnp.bfloat16), "tp", scatter_dimension=0, tiled=True
    ).astype(jnp.float32)
    layer_output = (hidden_state.astype(jnp.float32) + mixer_out).astype(jnp.bfloat16)
    return (layer_output, carried)


def solution(mesh):
    in_specs = (
        P("tp", "kv"),
        P("kv"),
        P("kv", "tp", None, None),
        P(),
        P("kv", "tp"),
        P("kv", "tp"),
        P("kv", "tp"),
        P("kv", "tp"),
        P("kv", "tp"),
        P("kv", "tp"),
        P("tp"),
        P(),
        P("tp", "kv"),
        P(),
        P("kv", "tp"),
        P("kv", "tp"),
        P("tp", "kv"),
    )
    out_specs = (P("tp", "kv"), P("kv", "tp", None, None))
    return jax.shard_map(local, mesh=mesh, in_specs=in_specs, out_specs=out_specs, check_vma=False)
```

profile of v0, /device:TPU:1, one launch (start us, length us, event | category | flops | bytes accessed | tf_op | source)
XLA Modules:
  0.0 607.4 jit_solution(7519099668961548802)
XLA Ops:
  7.2 7.4 %all_gather.12 = bf16[256,512]{1,0:T(8,128)(2,1)S(1)} all-gather(bf16[64,512]{1,0:T(8,128)(2,1)} %param.17), channel_id=1, replica_groups=mesh['kv'=8,'tp'=4] {'tp'}, dimensions={0}, use_global_device_ids=true | all-gather | bytes 327680 | tf_op jit(solution)/shard_map/all_gather | solution.py:55
  14.7 0.8 dynamic-slice_convert_fusion.1
  15.4 0.9 convolution_convert_fusion.8
  16.3 0.7 copy.112
  17.1 2.1 convolution_convert_fusion.6
  19.3 2.0 convolution_convert_fusion.5
  21.4 2.0 convolution_convert_fusion.7
  23.5 2.0 convolution_convert_fusion.4
  25.7 0.1 fusion.17
  25.8 0.6 dynamic-slice
  27.1 17.9 %all-reduce = bf16[256]{0:T(256)(128)(2,1)S(1)} all-reduce(bf16[256]{0:T(256)(128)(2,1)S(1)} %fusion.17), channel_id=3, replica_groups=mesh['kv'=8,'tp'=4] {'kv'}, use_global_device_ids=true, to_apply=%region_2.0.clone | all-reduce | flops 256 | bytes 1024
  45.1 33.3 %reduce-scatter.28.cloned.1.call-done = bf16[32,8]{1,0:T(8,128)(2,1)} async-done(((bf16[256,8]{1,0:T(8,128)(2,1)}), bf16[32,8]{1,0:T(8,128)(2,1)}) %reduce-scatter.28.cloned.1.call-update) | async-done | bytes 528
  78.4 0.8 copy.113
  79.3 0.1 fusion.40
  79.4 0.1 copy.93
  79.7 0.1 copy.78
  79.8 0.1 copy.79
  79.9 0.1 copy.81
  80.0 0.1 copy.84
  80.1 0.1 copy.86
  80.2 0.1 copy.89
  80.3 0.1 copy.94
  80.8 62.7 %reduce-scatter.14.cloned.1.call-done = bf16[32,512]{1,0:T(8,128)(2,1)} async-done(((bf16[256,512]{1,0:T(8,128)(2,1)}), bf16[32,512]{1,0:T(8,128)(2,1)}) %reduce-scatter.14.cloned.1.call-update) | async-done | bytes 32784 | tf_op jit(solution)/shard_map/reduce_scatter | solution.py:74
  143.5 64.4 %reduce-scatter.16.cloned.1.call-done = bf16[32,512]{1,0:T(8,128)(2,1)} async-done(((bf16[256,512]{1,0:T(8,128)(2,1)}), bf16[32,512]{1,0:T(8,128)(2,1)}) %reduce-scatter.16.cloned.1.call-update) | async-done | bytes 32784 | tf_op jit(solution)/shard_map/reduce_scatter | solution.py:77
  207.9 64.3 %reduce-scatter.12.cloned.1.call-done = bf16[32,512]{1,0:T(8,128)(2,1)} async-done(((bf16[256,512]{1,0:T(8,128)(2,1)}), bf16[32,512]{1,0:T(8,128)(2,1)}) %reduce-scatter.12.cloned.1.call-update) | async-done | bytes 32784 | tf_op jit(solution)/shard_map/reduce_scatter | solution.py:71
  272.2 0.9 convert_multiply_fusion.5
  273.1 0.1 multiply_reduce_fusion.1
  273.3 0.1 broadcast_multiply_fusion.1
  273.4 0.1 multiply_reduce_fusion.2
  273.6 0.1 multiply_multiply_fusion
  273.9 3.6 fusion.61
  277.5 2.1 fusion
  279.6 0.1 fusion.35
  279.7 2.9 fusion.56
  282.6 0.1 fusion.33
  282.7 3.8 fusion.2
  286.5 3.8 fusion.3
  290.4 2.9 fusion.57
  293.4 2.1 fusion.1
  295.6 0.1 fusion.31
  295.7 3.0 multiply_add_fusion
  298.8 1.3 copy-done.2
  300.0 1.9 fusion.62
  302.0 0.1 multiply_reduce_fusion
  302.1 0.1 broadcast_multiply_fusion
  302.2 34.3 %reduce-scatter.18.cloned.1.call-done = bf16[32,512]{1,0:T(8,128)(2,1)} async-done(((bf16[256,512]{1,0:T(8,128)(2,1)}), bf16[32,512]{1,0:T(8,128)(2,1)}) %reduce-scatter.18.cloned.1.call-update) | async-done | bytes 32784 | tf_op jit(solution)/shard_map/reduce_scatter | solution.py:80
  336.5 0.9 fusion.28
  337.4 25.1 %all_gather.13 = bf16[256,512]{1,0:T(8,128)(2,1)S(1)} all-gather(bf16[32,512]{1,0:T(8,128)(2,1)S(1)} %fusion.28), channel_id=1, replica_groups=mesh['kv'=8,'tp'=4] {'kv'}, dimensions={0}, use_global_device_ids=true | all-gather | bytes 294912 | tf_op jit(solution)/shard_map/all_gather | solution.py:114
  362.5 1.0 convolution_convert_fusion.3
  363.6 0.8 dynamic-slice_convert_fusion
  364.3 25.9 %reduce-scatter.20.cloned.1.call-done = bf16[64,512]{1,0:T(8,128)(2,1)} async-done(((bf16[256,512]{1,0:T(8,128)(2,1)}), bf16[64,512]{1,0:T(8,128)(2,1)}) %reduce-scatter.20.cloned.1.call-update) | async-done | bytes 65552 | tf_op jit(solution)/shard_map/reduce_scatter | solution.py:116
  390.2 0.9 add_convert_fusion.1
  391.1 6.5 %all_gather.14 = bf16[256,512]{1,0:T(8,128)(2,1)S(1)} all-gather(bf16[64,512]{1,0:T(8,128)(2,1)S(1)} %add_convert_fusion.1), channel_id=1, replica_groups=mesh['kv'=8,'tp'=4] {'tp'}, dimensions={0}, use_global_device_ids=true | all-gather | bytes 327680 | tf_op jit(solution)/shard_map/all_gather | solution.py:120
  397.6 2.0 convolution_convert_fusion
  399.7 3.9 convolution_convert_fusion.1
  403.6 0.1 fusion.18
  403.8 17.8 %all-reduce.1 = bf16[256]{0:T(256)(128)(2,1)S(1)} all-reduce(bf16[256]{0:T(256)(128)(2,1)S(1)} %fusion.18), channel_id=9, replica_groups=mesh['kv'=8,'tp'=4] {'kv'}, use_global_device_ids=true, to_apply=%region_12.13.clone | all-reduce | flops 256 | bytes 1024
  421.6 41.2 %reduce-scatter.24.cloned.1.call-done = bf16[32,2816]{1,0:T(8,128)(2,1)} async-done(((bf16[256,2816]{1,0:T(8,128)(2,1)}), bf16[32,2816]{1,0:T(8,128)(2,1)}) %reduce-scatter.24.cloned.1.call-update) | async-done | bytes 180240 | tf_op jit(solution)/shard_map/reduce_scatter | solution.py:133
  462.9 67.9 %reduce-scatter.22.cloned.1.call-done = bf16[32,2816]{1,0:T(8,128)(2,1)} async-done(((bf16[256,2816]{1,0:T(8,128)(2,1)}), bf16[32,2816]{1,0:T(8,128)(2,1)}) %reduce-scatter.22.cloned.1.call-update) | async-done | bytes 180240 | tf_op jit(solution)/shard_map/reduce_scatter | solution.py:130
  530.7 1.9 multiply_convert_fusion
  532.7 43.0 %all-gather.2.cloned.1.call-done = bf16[256,2816]{1,0:T(8,128)(2,1)} async-done(((bf16[32,2816]{1,0:T(8,128)(2,1)}), bf16[256,2816]{1,0:T(8,128)(2,1)}) %all-gather.2.cloned.1.call-update) | async-done | bytes 1441808 | tf_op jit(solution)/shard_map/all_gather | solution.py:145
  575.6 3.9 convolution_convert_fusion.2
  579.5 19.6 %reduce-scatter.26.cloned.1.call-done = bf16[64,512]{1,0:T(8,128)(2,1)} async-done(((bf16[256,512]{1,0:T(8,128)(2,1)}), bf16[64,512]{1,0:T(8,128)(2,1)}) %reduce-scatter.26.cloned.1.call-update) | async-done | bytes 65552 | tf_op jit(solution)/shard_map/reduce_scatter | solution.py:149
  599.1 1.5 add_convert_fusion
  (72 shorter events, 2.2 us)
Async XLA Ops:
  7.2 390.4 %copy-start = (bf16[512,2816]{1,0:T(8,128)(2,1)S(1)}, bf16[512,2816]{1,0:T(8,128)(2,1)}, u32[]{:S(2)}) copy-start(bf16[512,2816]{1,0:T(8,128)(2,1)} %param.32) | copy-start | bytes 8650756
  7.2 71.2 %reduce-scatter.28.cloned.1.call-start = ((), (), s32[]{:S(2)}) async-start(), calls=%async_computation.18 | async-start | bytes 73728
  17.1 126.4 %reduce-scatter.14.cloned.1.call-start = ((), (), s32[]{:S(2)}) async-start(), calls=%async_computation.10 | async-start | bytes 294912 | tf_op jit(solution)/shard_map/reduce_scatter | solution.py:74
  19.2 6.6 %copy-start.8 = (u32[32]{0:T(128)S(1)}, u32[32]{0:T(128)}, u32[]{:S(2)}) copy-start(u32[32]{0:T(128)} %constant.39) | copy-start | bytes 388
  19.2 7.8 %copy-start.7 = (f32[4]{0:T(128)S(1)}, f32[4]{0:T(128)}, u32[]{:S(2)}) copy-start(f32[4]{0:T(128)} %param.27) | copy-start | bytes 52
  19.2 7.9 %copy-start.5 = (s32[8]{0:T(128)S(1)}, s32[8]{0:T(128)}, u32[]{:S(2)}) copy-start(s32[8]{0:T(128)} %param.18) | copy-start | bytes 100
  19.2 7.9 %copy-start.6 = (f32[128]{0:T(128)S(1)}, f32[128]{0:T(128)}, u32[]{:S(2)}) copy-start(f32[128]{0:T(128)} %param.28) | copy-start | bytes 1540
  19.3 188.7 %reduce-scatter.16.cloned.1.call-start = ((), (), s32[]{:S(2)}) async-start(), calls=%async_computation.11 | async-start | bytes 294912 | tf_op jit(solution)/shard_map/reduce_scatter | solution.py:77
  21.4 250.9 %reduce-scatter.12.cloned.1.call-start = ((), (), s32[]{:S(2)}) async-start(), calls=%async_computation.9 | async-start | bytes 294912 | tf_op jit(solution)/shard_map/reduce_scatter | solution.py:71
  23.5 313.0 %reduce-scatter.18.cloned.1.call-start = ((), (), s32[]{:S(2)}) async-start(), calls=%async_computation.12 | async-start | bytes 294912 | tf_op jit(solution)/shard_map/reduce_scatter | solution.py:80
  25.6 364.6 %reduce-scatter.20.cloned.1.call-start = ((), (), s32[]{:S(2)}) async-start(), calls=%async_computation.13 | async-start | bytes 327680 | tf_op jit(solution)/shard_map/reduce_scatter | solution.py:116
  273.8 3.7 copy-start.1
  298.7 1.3 copy-start.2
  298.7 63.8 %copy-start.3 = (bf16[512,512]{1,0:T(8,128)(2,1)S(1)}, bf16[512,512]{1,0:T(8,128)(2,1)}, u32[]{:S(2)}) copy-start(bf16[512,512]{1,0:T(8,128)(2,1)} %param.29) | copy-start | bytes 1572868
  298.7 91.5 %copy-start.4 = (bf16[64,512]{1,0:T(8,128)(2,1)S(1)}, bf16[64,512]{1,0:T(8,128)(2,1)}, u32[]{:S(2)}) copy-start(bf16[64,512]{1,0:T(8,128)(2,1)} %param.17) | copy-start | bytes 196612
  363.5 99.3 %reduce-scatter.24.cloned.1.call-start = ((), (), s32[]{:S(2)}) async-start(), calls=%async_computation.15 | async-start | bytes 1622016 | tf_op jit(solution)/shard_map/reduce_scatter | solution.py:133
  399.7 131.1 %reduce-scatter.22.cloned.1.call-start = ((), (), s32[]{:S(2)}) async-start(), calls=%async_computation.14 | async-start | bytes 1622016 | tf_op jit(solution)/shard_map/reduce_scatter | solution.py:130
  403.6 172.0 %all-gather.2.cloned.1.call-start = ((), (), s32[]{:S(2)}) async-start(), calls=%async_computation.16 | async-start | bytes 1622016 | tf_op jit(solution)/shard_map/all_gather | solution.py:145
  532.6 66.5 %reduce-scatter.26.cloned.1.call-start = ((), (), s32[]{:S(2)}) async-start(), calls=%async_computation.17 | async-start | bytes 327680 | tf_op jit(solution)/shard_map/reduce_scatter | solution.py:149
Sparse Core Ops, SparseCore 0:
  17.2 61.1 reduce-scatter.27
  82.3 61.1 reduce-scatter.13
  146.8 61.0 reduce-scatter.15
  211.1 61.0 reduce-scatter.11
  275.4 61.0 reduce-scatter.17
  363.6 26.5 reduce-scatter.19
  399.8 63.0 reduce-scatter.23
  466.3 64.3 reduce-scatter.21
  532.9 42.6 all-gather.1
  579.6 19.4 reduce-scatter.25
where the time goes:
time: 609 us; the launch traced here: 607 us
  waiting for transfers between devices  457 us (75%)
  blocking collectives  74.8 us (12%)
  matrix products  42.9 us (7%)
  between operations  15.1 us (2%)
  other arithmetic  12.5 us (2%)
    reduce_scatter x1, waiting for transfers between devices, local(): lax.psum_scatter(gate_terms.astype(jnp.bfloat16), 'kv', scatter_dimension...  67.9 us
    reduce_scatter x1, waiting for transfers between devices, local(): lax.psum_scatter(value_part.astype(jnp.bfloat16), 'kv', scatter_dimension...  64.4 us
    reduce_scatter x1, waiting for transfers between devices, local(): lax.psum_scatter(query_part.astype(jnp.bfloat16), 'kv', scatter_dimension...  64.3 us
    reduce_scatter x1, waiting for transfers between devices, local(): lax.psum_scatter(key_part.astype(jnp.bfloat16), 'kv', scatter_dimension=0...  62.7 us
    all_gather x1, waiting for transfers between devices, local(): lax.all_gather(activated, 'kv', axis=0, tiled=True)  43 us
    reduce_scatter x1, waiting for transfers between devices, local(): lax.psum_scatter(up_terms.astype(jnp.bfloat16), 'kv', scatter_dimension=0...  41.2 us
    unnamed x2, blocking collectives  35.7 us
    reduce_scatter x1, waiting for transfers between devices, local(): lax.psum_scatter(gate_part.astype(jnp.bfloat16), 'kv', scatter_dimension=...  34.3 us
  transfers between devices with their start and end apart: 10, of which 10 were waited for; matrix products, arithmetic and copies ran while one was open for 7% of the time, Pallas kernels for 0%

commit v1 on v0

v1 whole, which is shorter than its diff:
```python
import functools

import jax
import jax.numpy as jnp
from jax import lax
from jax.experimental import pallas as pl
from jax.experimental.pallas import tpu as pltpu
from jax.sharding import PartitionSpec as P

MESH = pl.DeviceIdType.MESH
D = 4096
NEW = 4
EPS = 1e-06
LANES = 128
F32 = jnp.float32
BF16 = jnp.bfloat16


def grid_of(n_kv):
    nx = 1
    while nx * nx * 8 <= n_kv:
        nx *= 2
    return n_kv // nx, nx


def groups_of(width, count):
    units = width // LANES
    count = min(count, units)
    sizes = [units // count + (1 if i < units % count else 0) for i in range(count)]
    spans, at = [], 0
    for size in sizes:
        spans.append((at * LANES, size * LANES))
        at += size
    return spans


class Net:
    def __init__(self, n_kv, n_tp, send_sem, recv_sem):
        self.n_kv, self.n_tp = n_kv, n_tp
        self.nz, self.nx = grid_of(n_kv)
        self.kv, self.tp = lax.axis_index("kv"), lax.axis_index("tp")
        self.z, self.x = self.kv // self.nx, self.kv % self.nx
        self.send_sem, self.recv_sem = send_sem, recv_sem
        self.started = []

    def tp_peer(self, d):
        return (self.tp + d) % self.n_tp

    def kv_peer(self, d):
        return (self.kv + d) % self.n_kv

    def z_peer(self, d):
        return (self.z + d) % self.nz

    def x_peer(self, d):
        return (self.x + d) % self.nx

    def barrier(self):
        sem = pltpu.get_barrier_semaphore()
        for d in range(1, self.n_tp):
            pl.semaphore_signal(
                sem, inc=1, device_id={"kv": self.kv, "tp": self.tp_peer(d)}, device_id_type=MESH
            )
        for d in range(1, self.n_kv):
            pl.semaphore_signal(
                sem, inc=1, device_id={"kv": self.kv_peer(d), "tp": self.tp}, device_id_type=MESH
            )
        pl.semaphore_wait(sem, self.n_tp + self.n_kv - 2)

    def send(self, src, dst, kv, tp):
        at = len(self.started)
        copy = pltpu.make_async_remote_copy(
            src_ref=src,
            dst_ref=dst,
            send_sem=self.send_sem.at[at],
            recv_sem=self.recv_sem.at[at],
            device_id={"kv": kv, "tp": tp},
            device_id_type=MESH,
        )
        copy.start()
        self.started.append(copy)
        return copy

    def drain(self):
        for copy in self.started:
            copy.wait_send()


def arrive(copies):
    for copy in copies:
        copy.wait_recv()


def gather_tp(net, src, dst):
    return [net.send(src, dst.at[net.tp], net.kv, net.tp_peer(d)) for d in range(1, net.n_tp)]


def scatter_tp(net, src, dst):
    return [
        net.send(src.at[net.tp_peer(d)], dst.at[d - 1], net.kv, net.tp_peer(d))
        for d in range(1, net.n_tp)
    ]


def gather_kv(net, src, dst):
    return [net.send(src, dst.at[net.kv], net.kv_peer(d), net.tp) for d in range(1, net.n_kv)]


def scatter_kv(net, src, dst):
    return [
        net.send(src.at[net.kv_peer(d)], dst.at[d - 1], net.kv_peer(d), net.tp)
        for d in range(1, net.n_kv)
    ]


def scatter_x(net, parts, got, cols):
    return [
        net.send(
            parts.at[net.x_peer(d), :, cols],
            got.at[d - 1, :, cols],
            net.z * net.nx + net.x_peer(d),
            net.tp,
        )
        for d in range(1, net.nx)
    ]


def scatter_z(net, parts, got, cols):
    return [
        net.send(
            parts.at[net.z_peer(d), :, cols],
            got.at[d - 1, :, cols],
            net.z_peer(d) * net.nx + net.x,
            net.tp,
        )
        for d in range(1, net.nz)
    ]


def store_parts(net, parts, product, cols):
    own = product.shape[0] // net.n_kv
    for block in range(net.n_kv):
        z, x = block // net.nx, block % net.nx
        parts[x, z * own : (z + 1) * own, cols] = product[block * own : (block + 1) * own].astype(
            BF16
        )


def fold_x(net, parts, got, folded, cols):
    total = parts[net.x, :, cols].astype(F32)
    for d in range(1, net.nx):
        total = total + got[d - 1, :, cols].astype(F32)
    folded[:, :, cols] = total.astype(BF16).reshape(net.nz, -1, total.shape[1])


def fold_z(net, folded, got, cols):
    total = folded[net.z, :, cols].astype(F32)
    for d in range(1, net.nz):
        total = total + got[d - 1, :, cols].astype(F32)
    return total


def project_kernel(
    n_kv,
    n_tp,
    x_ref,
    gain_ref,
    rate_ref,
    wq_hbm,
    wk_hbm,
    wv_hbm,
    wo_hbm,
    out_ref,
    aux_out_ref,
    weights,
    x_all,
    aux,
    aux_got,
    parts,
    x_got,
    folded,
    z_got,
    load_sem,
    send_sem,
    recv_sem,
):
    net = Net(n_kv, n_tp, send_sem, recv_sem)
    loads = []
    for i, source in enumerate((wq_hbm, wk_hbm, wv_hbm, wo_hbm)):
        copy = pltpu.make_async_copy(source, weights.at[i], load_sem.at[i])
        copy.start()
        loads.append(copy)
    net.barrier()
    incoming = gather_tp(net, x_ref, x_all)
    x_all[net.tp] = x_ref[...]
    arrive(incoming)
    wide = x_all[...].reshape(-1, x_ref.shape[1]).astype(F32)
    squares = jnp.sum(wide * wide, axis=1, keepdims=True)
    normed = (wide * gain_ref[net.kv]).astype(BF16)
    rates = jnp.dot(normed, rate_ref[...], preferred_element_type=F32)
    lane = lax.broadcasted_iota(jnp.int32, rates.shape, 1)
    aux[...] = jnp.where(lane == LANES - 1, squares, rates).reshape(aux.shape)
    aux_in = scatter_kv(net, aux, aux_got)
    width = weights.shape[2]
    crossing = []
    for i in range(4):
        cols = pl.ds(i * width, width)
        loads[i].wait()
        product = jnp.dot(normed, weights[i], preferred_element_type=F32)
        store_parts(net, parts, product, cols)
        crossing.append(scatter_x(net, parts, x_got, cols))
    climbing = []
    for i in range(4):
        cols = pl.ds(i * width, width)
        arrive(crossing[i])
        fold_x(net, parts, x_got, folded, cols)
        climbing.append(scatter_z(net, folded, z_got, cols))
    arrive(aux_in)
    aux_out_ref[...] = aux[net.kv] + jnp.sum(aux_got[...], axis=0)
    for i in range(4):
        cols = pl.ds(i * width, width)
        arrive(climbing[i])
        out_ref[:, cols] = fold_z(net, folded, z_got, cols)
    net.drain()


def mixer_kernel(
    n_kv,
    n_tp,
    n_groups,
    mixed_ref,
    x_ref,
    gain_ref,
    w_out_hbm,
    w_gate_hbm,
    w_up_hbm,
    w_down_hbm,
    out_ref,
    w_out,
    w_gate,
    w_up,
    w_down,
    mixed_all,
    out_parts,
    out_got,
    hidden_all,
    aux,
    aux_got,
    parts,
    x_got,
    folded,
    z_got,
    act,
    down_parts,
    down_got,
    load_sem,
    send_sem,
    recv_sem,
):
    net = Net(n_kv, n_tp, send_sem, recv_sem)
    loads = []
    pairs = ((w_out_hbm, w_out), (w_gate_hbm, w_gate), (w_up_hbm, w_up), (w_down_hbm, w_down))
    for i, (source, target) in enumerate(pairs):
        copy = pltpu.make_async_copy(source, target, load_sem.at[i])
        copy.start()
        loads.append(copy)
    net.barrier()
    incoming = gather_kv(net, mixed_ref, mixed_all)
    mixed_all[net.kv] = mixed_ref[...]
    arrive(incoming)
    loads[0].wait()
    terms = jnp.dot(
        mixed_all[...].reshape(-1, mixed_ref.shape[1]), w_out[...], preferred_element_type=F32
    )
    out_parts[...] = terms.astype(BF16).reshape(out_parts.shape)
    arrive(scatter_tp(net, out_parts, out_got))
    attended = out_parts[net.tp].astype(F32)
    for d in range(1, n_tp):
        attended = attended + out_got[d - 1].astype(F32)
    hidden = (x_ref[...].astype(F32) + attended).astype(BF16)
    hidden_all[net.tp] = hidden
    arrive(gather_tp(net, hidden_all.at[net.tp], hidden_all))
    wide = hidden_all[...].reshape(-1, x_ref.shape[1]).astype(F32)
    squares = jnp.sum(wide * wide, axis=1, keepdims=True)
    normed = (wide * gain_ref[net.kv]).astype(BF16)
    aux[...] = jnp.broadcast_to(squares, (squares.shape[0], LANES)).reshape(aux.shape)
    aux_in = scatter_kv(net, aux, aux_got)
    spans = groups_of(w_gate.shape[1], n_groups)
    count = len(spans)
    crossing, climbing, rising, spreading = [], [], [], []
    loads[1].wait()
    loads[2].wait()
    for at, size in spans:
        store_parts(
            net,
            parts,
            jnp.dot(normed, w_gate[:, pl.ds(at, size)], preferred_element_type=F32),
            pl.ds(2 * at, size),
        )
        store_parts(
            net,
            parts,
            jnp.dot(normed, w_up[:, pl.ds(at, size)], preferred_element_type=F32),
            pl.ds(2 * at + size, size),
        )
        crossing.append(scatter_x(net, parts, x_got, pl.ds(2 * at, 2 * size)))
    arrive(aux_in)
    total = aux[net.kv]
    for d in range(1, n_kv):
        total = total + aux_got[d - 1]
    scale = lax.rsqrt(total[:, :1] / D + EPS)
    loads[3].wait()
    down = None
    for step in range(count + 3):
        if step < count:
            at, size = spans[step]
            cols = pl.ds(2 * at, 2 * size)
            arrive(crossing[step])
            fold_x(net, parts, x_got, folded, cols)
            climbing.append(scatter_z(net, folded, z_got, cols))
        if 0 <= step - 1 < count:
            at, size = spans[step - 1]
            arrive(climbing[step - 1])
            gate = fold_z(net, folded, z_got, pl.ds(2 * at, size)) * scale
            up = fold_z(net, folded, z_got, pl.ds(2 * at + size, size)) * scale
            act[net.z, net.x, :, pl.ds(at, size)] = (jax.nn.silu(gate) * up).astype(BF16)
            block = act.at[net.z, net.x, :, pl.ds(at, size)]
            rising.append(
                [
                    net.send(block, block, net.z_peer(d) * net.nx + net.x, net.tp)
                    for d in range(1, net.nz)
                ]
            )
        if 0 <= step - 2 < count:
            at, size = spans[step - 2]
            arrive(rising[step - 2])
            block = act.at[:, net.x, :, pl.ds(at, size)]
            spreading.append(
                [
                    net.send(block, block, net.z * net.nx + net.x_peer(d), net.tp)
                    for d in range(1, net.nx)
                ]
            )
        if 0 <= step - 3 < count:
            at, size = spans[step - 3]
            arrive(spreading[step - 3])
            block = act[:, :, :, pl.ds(at, size)].reshape(-1, size)
            term = jnp.dot(block, w_down[pl.ds(at, size), :], preferred_element_type=F32)
            down = term if down is None else down + term
    down_parts[...] = down.astype(BF16).reshape(down_parts.shape)
    arrive(scatter_tp(net, down_parts, down_got))
    result = down_parts[net.tp].astype(F32)
    for d in range(1, n_tp):
        result = result + down_got[d - 1].astype(F32)
    out_ref[...] = (hidden_all[net.tp].astype(F32) + result).astype(BF16)
    net.drain()


def vmem():
    return pl.BlockSpec(memory_space=pltpu.VMEM)


def hbm():
    return pl.BlockSpec(memory_space=pl.ANY)


def params(collective_id):
    return pltpu.CompilerParams(
        collective_id=collective_id, has_side_effects=True, vmem_limit_bytes=56 * 1024 * 1024
    )


def unit_norm(vectors):
    return vectors * lax.rsqrt(jnp.sum(vectors * vectors, axis=-1, keepdims=True) + EPS)


def run_delta(carried, query_unit, key_unit, value_act, write_rate, log_keep, live):
    readings = []
    for position in range(query_unit.shape[1]):
        active = live[:, position][:, None]
        beta = write_rate[:, position] * active
        keep = jnp.exp(log_keep[:, position] * active)
        key_now = key_unit[:, position]
        recalled = jnp.einsum("shk,shkv->shv", key_now, carried, precision=lax.Precision.HIGHEST)
        update = beta[:, :, None] * (value_act[:, position] - keep[:, :, None] * recalled)
        carried = keep[:, :, None, None] * carried + key_now[:, :, :, None] * update[:, :, None, :]
        reading = jnp.einsum(
            "shk,shkv->shv", query_unit[:, position], carried, precision=lax.Precision.HIGHEST
        )
        readings.append(reading * active[:, :, None])
    return (carried, jnp.stack(readings, axis=1))


def local(
    n_kv,
    n_tp,
    layer_input,
    seq_lengths,
    delta_state,
    attn_gain,
    w_query,
    w_key,
    w_value,
    w_outgate,
    w_write,
    w_forget,
    forget_rate,
    head_gain,
    w_out,
    mixer_gain,
    w_gate,
    w_up,
    w_down,
):
    tp_rows, features = layer_input.shape
    rows = tp_rows * n_tp
    own = rows // n_kv
    nz, nx = grid_of(n_kv)
    head_cols = w_query.shape[1]
    seqs_here = seq_lengths.shape[0]
    heads_here = forget_rate.shape[0]
    head_size = head_gain.shape[0]
    rate_weight = jnp.pad(
        jnp.concatenate([w_write, w_forget], axis=1), ((0, 0), (0, LANES - 2 * heads_here))
    )
    copies = (n_tp - 1) + (n_kv - 1) + 4 * (nx - 1 + nz - 1)
    sums, aux = pl.pallas_call(
        functools.partial(project_kernel, n_kv, n_tp),
        out_shape=(
            jax.ShapeDtypeStruct((own, 4 * head_cols), F32),
            jax.ShapeDtypeStruct((own, LANES), F32),
        ),
        in_specs=[vmem()] * 3 + [hbm()] * 4,
        out_specs=(vmem(), vmem()),
        scratch_shapes=[
            pltpu.VMEM((4, features, head_cols), BF16),
            pltpu.VMEM((n_tp, tp_rows, features), BF16),
            pltpu.VMEM((n_kv, own, LANES), F32),
            pltpu.VMEM((n_kv - 1, own, LANES), F32),
            pltpu.VMEM((nx, nz * own, 4 * head_cols), BF16),
            pltpu.VMEM((nx - 1, nz * own, 4 * head_cols), BF16),
            pltpu.VMEM((nz, own, 4 * head_cols), BF16),
            pltpu.VMEM((nz - 1, own, 4 * head_cols), BF16),
            pltpu.SemaphoreType.DMA((4,)),
            pltpu.SemaphoreType.DMA((copies,)),
            pltpu.SemaphoreType.DMA((copies,)),
        ],
        compiler_params=params(0),
    )(
        layer_input,
        attn_gain.astype(F32).reshape(n_kv, 1, features),
        rate_weight,
        w_query,
        w_key,
        w_value,
        w_outgate,
    )
    row_scale = lax.rsqrt(aux[:, LANES - 1 :] / D + EPS)

    def split_heads(at):
        block = sums[:, at * head_cols : (at + 1) * head_cols]
        return (block * row_scale).reshape(seqs_here, NEW, heads_here, head_size)

    query_unit = unit_norm(jax.nn.silu(split_heads(0))) * head_size ** (-0.5)
    key_unit = unit_norm(jax.nn.silu(split_heads(1)))
    value_act = jax.nn.silu(split_heads(2))
    outgate = split_heads(3)
    rate_rows = (aux[:, : 2 * heads_here] * row_scale).reshape(seqs_here, NEW, 2 * heads_here)
    write_rate = jax.nn.sigmoid(rate_rows[:, :, :heads_here])
    log_keep = -forget_rate * jax.nn.softplus(rate_rows[:, :, heads_here:])
    positions = jnp.arange(NEW, dtype=jnp.int32)
    live = (positions[None, :] < seq_lengths[:, None]).astype(F32)
    carried, readings = run_delta(
        delta_state, query_unit, key_unit, value_act, write_rate, log_keep, live
    )
    normed = readings * lax.rsqrt(jnp.mean(readings * readings, axis=-1, keepdims=True) + EPS)
    normed = normed * head_gain * jax.nn.silu(outgate)
    mixed = normed.reshape(own, heads_here * head_size).astype(BF16)

    hidden_cols = w_gate.shape[1]
    n_groups = 6
    groups = len(groups_of(hidden_cols, n_groups))
    copies = 3 * (n_tp - 1) + 2 * (n_kv - 1) + 2 * groups * (nx - 1 + nz - 1)
    layer_output = pl.pallas_call(
        functools.partial(mixer_kernel, n_kv, n_tp, n_groups),
        out_shape=jax.ShapeDtypeStruct((tp_rows, features), BF16),
        in_specs=[vmem()] * 3 + [hbm()] * 4,
        out_specs=vmem(),
        scratch_shapes=[
            pltpu.VMEM(w_out.shape, BF16),
            pltpu.VMEM(w_gate.shape, BF16),
            pltpu.VMEM(w_up.shape, BF16),
            pltpu.VMEM(w_down.shape, BF16),
            pltpu.VMEM((n_kv, own, head_cols), BF16),
            pltpu.VMEM((n_tp, tp_rows, features), BF16),
            pltpu.VMEM((n_tp - 1, tp_rows, features), BF16),
            pltpu.VMEM((n_tp, tp_rows, features), BF16),
            pltpu.VMEM((n_kv, own, LANES), F32),
            pltpu.VMEM((n_kv - 1, own, LANES), F32),
            pltpu.VMEM((nx, nz * own, 2 * hidden_cols), BF16),
            pltpu.VMEM((nx - 1, nz * own, 2 * hidden_cols), BF16),
            pltpu.VMEM((nz, own, 2 * hidden_cols), BF16),
            pltpu.VMEM((nz - 1, own, 2 * hidden_cols), BF16),
            pltpu.VMEM((nz, nx, own, hidden_cols), BF16),
            pltpu.VMEM((n_tp, tp_rows, features), BF16),
            pltpu.VMEM((n_tp - 1, tp_rows, features), BF16),
            pltpu.SemaphoreType.DMA((4,)),
            pltpu.SemaphoreType.DMA((copies,)),
            pltpu.SemaphoreType.DMA((copies,)),
        ],
        compiler_params=params(1),
    )(
        mixed,
        layer_input,
        mixer_gain.astype(F32).reshape(n_kv, 1, features),
        w_out,
        w_gate,
        w_up,
        w_down,
    )
    return (layer_output, carried)


def solution(mesh):
    in_specs = (
        P("tp", "kv"),
        P("kv"),
        P("kv", "tp", None, None),
        P(),
        P("kv", "tp"),
        P("kv", "tp"),
        P("kv", "tp"),
        P("kv", "tp"),
        P("kv", "tp"),
        P("kv", "tp"),
        P("tp"),
        P(),
        P("tp", "kv"),
        P(),
        P("kv", "tp"),
        P("kv", "tp"),
        P("tp", "kv"),
    )
    out_specs = (P("tp", "kv"), P("kv", "tp", None, None))
    body = functools.partial(local, mesh.shape["kv"], mesh.shape["tp"])
    return jax.shard_map(body, mesh=mesh, in_specs=in_specs, out_specs=out_specs, check_vma=False)
```

time: 609 us -> 155 us (0.25)
  waiting for transfers between devices: 457 us -> 0 us
  Pallas kernels: 0 us -> 118 us
  blocking collectives: 74.8 us -> 0 us
  matrix products: 42.9 us -> 21.6 us
  between operations: 15.1 us -> 0.93 us
    reduce_scatter x8 -> x0, waiting for transfers between devices: 380 us -> none  [the longest x1 67.9 us: local(): lax.psum_scatter(gate_terms.astype(jnp.bfloat16), 'kv', scatter_dimension...]
    pallas_call x0 -> x2, Pallas kernels: none -> 118 us  [the longest x1 88.5 us: local(): pl.pallas_call(functools.partial(mixer_kernel, n_kv, n_tp, n_groups), out...]
    all_gather x1 -> x0, waiting for transfers between devices: 43 us -> none  [local(): lax.all_gather(activated, 'kv', axis=0, tiled=True)]
    all_gather x3 -> x0, blocking collectives: 39.1 us -> none  [the longest x1 25.1 us: local(): lax.all_gather(mixed, 'kv', axis=0, tiled=True)]
    unnamed x2 -> x0, blocking collectives: 35.7 us -> none
    unnamed x11 -> x0, waiting for transfers between devices: 33.4 us -> none
    dot_general x9 -> x0, matrix products: 19.8 us -> none  [the longest x1 3.86 us: local(): jnp.dot(lax.all_gather(activated, 'kv', axis=0, tiled=True), w_down, pref...]
  transfers between devices with their start and end apart: 10 -> 0, of which waited for: 10 -> 0; matrix products, arithmetic and copies ran while one was open for 7% -> 0% of each run, Pallas kernels for 0% -> 0%
where the time goes in v1:
time: 155 us
  Pallas kernels  118 us (76%)
  matrix products  21.6 us (14%)
  other arithmetic  11.3 us (7%)
  local copies, waits for them, and re-layouts  3.4 us (2%)
    pallas_call x1, Pallas kernels, local(): pl.pallas_call(functools.partial(mixer_kernel, n_kv, n_tp, n_groups), out...  88.5 us
    pallas_call x1, Pallas kernels, local(): pl.pallas_call(functools.partial(project_kernel, n_kv, n_tp), out_shape=(...  29.2 us
    dot_general x4, matrix products, run_delta(): jnp.einsum('shk,shkv->shv', query_unit[:, position], carried, precision=l...  10.9 us
    dot_general x4, matrix products, run_delta(): jnp.einsum('shk,shkv->shv', key_now, carried, precision=lax.Precision.HIG...  10.7 us

profile of v1, /device:TPU:1, one launch (start us, length us, event | category | flops | bytes accessed | tf_op | source)
XLA Modules:
  0.0 154.9 jit_solution(9474720241818253971)
XLA Ops:
  0.6 0.0 copy-start
  0.6 0.0 copy-start.5
  0.7 0.0 copy-start.4
  0.7 0.0 copy-start.1
  0.7 0.9 pad_maximum_fusion.1
  1.5 0.2 copy.51
  1.7 0.7 pad.4.rate_ref
  2.4 1.3 reshape.335
  3.7 29.2 %shard_map.176 = (f32[32,2048]{1,0:T(8,128)}, f32[32,128]{1,0:T(8,128)}) custom-call(bf16[64,512]{1,0:T(8,128)(2,1)} %x_ref.3, f32[8,1,512]{2,1,0:T(1,128)} %bitcast.161, bf16[512,128]{1,0:T(8,128)(2,1)} %pad.4.rate_ref, bf16[512,512]{1,0:T(8,128)(2,1)} %wq_hbm.1, bf16[512,512]{1,0:T(8,128)(2,1)} %wk_hbm.1, bf16[512,512]{1,0:T(8,128)(2,1)} %wv_hbm.1, ...), custom_call_target="tpu_custom_call" | custom-call | tf_op jit(solution)/shard_map/pallas_call | solution.py:427
  32.9 0.9 rsqrt_reduce_fusion
  33.8 0.8 slice_multiply_fusion.3
  34.6 0.1 fusion.43
  34.7 0.1 copy.82
  34.8 0.0 copy-done.5
  34.8 0.1 fusion.26
  34.9 0.1 copy.83
  35.0 0.0 copy-done.4
  35.1 0.1 copy.53
  35.2 0.1 copy.55
  35.3 1.0 slice_multiply_fusion.1
  36.3 0.1 multiply_reduce_fusion.1
  36.4 0.1 broadcast_multiply_fusion.1
  36.6 0.0 copy-done.1
  36.6 1.9 %fusion.44 = f32[8,4,1,128]{3,2,1,0:T(1,128)S(1)} fusion(f32[8,4,128,1]{2,3,1,0:T(1,128)S(1)} %bitcast.158, f32[8,4,128,128]{3,2,1,0:T(8,128)S(1)} %copy-done.1), kind=kOutput, calls=%fused_computation.96 | convolution fusion | flops 6291456 | bytes 2129920 | tf_op jit(solution)/shard_map/shk,shkv->shv/dot_general | solution.py:384
  38.5 0.1 fusion.25
  38.7 0.1 multiply_reduce_fusion.2
  38.8 0.1 multiply_multiply_fusion
  39.0 2.1 %fusion.1 = f32[8,4,1,128]{3,2,1,0:T(1,128)S(1)} fusion(f32[8,4,128,1]{2,3,1,0:T(1,128)S(1)} %bitcast.166, f32[8,4,128,128]{3,2,1,0:T(8,128)S(1)} %copy-done.1, f32[8,4,128]{2,1,0:T(4,128)S(1)} %fusion.25, f32[8,4,128]{2,1,0:T(4,128)S(1)} %get-tuple-element.14, f32[8,4]{1,0:T(8,128)S(1)} %copy.53), kind=kOutput, calls=%fused_computation.5 | convolution fusion | flops 7864320 | bytes 2162816 | tf_op jit(solution)/shard_map/shk,shkv->shv/dot_general | solution.py:387
  41.1 2.1 %fusion = f32[8,4,1,128]{3,2,1,0:T(1,128)S(1)} fusion(f32[8,4,128,1]{2,3,1,0:T(1,128)S(1)} %bitcast.157, f32[8,4,128,128]{3,2,1,0:T(8,128)S(1)} %copy-done.1, f32[8,4,128]{2,1,0:T(4,128)S(1)} %fusion.25, f32[8,4,128]{2,1,0:T(4,128)S(1)} %get-tuple-element.14, f32[8,4]{1,0:T(8,128)S(1)} %copy.53), kind=kOutput, calls=%fused_computation.4 | convolution fusion | flops 7864320 | bytes 2162816 | tf_op jit(solution)/shard_map/shk,shkv->shv/dot_general | solution.py:384
  43.2 0.1 copy.57
  43.2 0.1 copy.58
  43.3 0.1 fusion.23
  43.4 3.1 %fusion.41 = f32[8,4,1,128]{3,2,1,0:T(1,128)S(1)} fusion(f32[8,4,128,1]{2,3,1,0:T(1,128)S(1)} %bitcast.174, f32[8,4,128,128]{3,2,1,0:T(8,128)S(1)} %copy-done.1, f32[8,4,128]{2,1,0:T(4,128)S(1)} %fusion.23, f32[8,4,128]{2,1,0:T(4,128)S(1)} %get-tuple-element.15, f32[8,4]{1,0:T(8,128)S(1)} %copy.57, f32[8,4,128]{2,1,0:T(4,128)S(1)} %fusion.25, ...), kind=kOutput, calls=%fused_computation.93 | convolution fusion | flops 9437184 | bytes 2195712 | tf_op jit(solution)/shard_map/shk,shkv->shv/dot_general | solution.py:387
  46.5 0.1 multiply_bitcast_fusion.2
  46.6 2.9 %fusion.40 = f32[8,4,1,128]{3,2,1,0:T(1,128)S(1)} fusion(f32[8,4,128,1]{2,3,1,0:T(1,128)S(1)} %bitcast.168, f32[8,4,128,128]{3,2,1,0:T(8,128)S(1)} %copy-done.1, f32[8,4,128]{2,1,0:T(4,128)S(1)} %fusion.23, f32[8,4,128]{2,1,0:T(4,128)S(1)} %get-tuple-element.15, f32[8,4]{1,0:T(8,128)S(1)} %copy.57, f32[8,4,128]{2,1,0:T(4,128)S(1)} %fusion.25, ...), kind=kOutput, calls=%fused_computation.92 | convolution fusion | flops 9437184 | bytes 2195712 | tf_op jit(solution)/shard_map/shk,shkv->shv/dot_general | solution.py:384
  49.5 0.1 copy.60
  49.5 0.1 copy.61
  49.6 0.1 fusion.21
  49.7 3.8 %fusion.3 = f32[8,4,1,128]{3,2,1,0:T(1,128)S(1)} fusion(f32[8,4,128,1]{2,3,1,0:T(1,128)S(1)} %bitcast.173, f32[8,4,128]{2,1,0:T(4,128)S(1)} %fusion.21, f32[8,4,128]{2,1,0:T(4,128)S(1)} %get-tuple-element.16, f32[8,4]{1,0:T(8,128)S(1)} %copy.60, f32[8,4,128,128]{3,2,1,0:T(8,128)S(1)} %copy-done.1, f32[8,4,128]{2,1,0:T(4,128)S(1)} %fusion.23, ...), kind=kOutput, calls=%fused_computation.7 | convolution fusion | flops 11010048 | bytes 2228608 | tf_op jit(solution)/shard_map/shk,shkv->shv/dot_general | solution.py:387
  53.6 3.8 %fusion.2 = f32[8,4,1,128]{3,2,1,0:T(1,128)S(1)} fusion(f32[8,4,128,1]{2,3,1,0:T(1,128)S(1)} %bitcast.167, f32[8,4,128]{2,1,0:T(4,128)S(1)} %fusion.21, f32[8,4,128]{2,1,0:T(4,128)S(1)} %get-tuple-element.16, f32[8,4]{1,0:T(8,128)S(1)} %copy.60, f32[8,4,128,128]{3,2,1,0:T(8,128)S(1)} %copy-done.1, f32[8,4,128]{2,1,0:T(4,128)S(1)} %fusion.23, ...), kind=kOutput, calls=%fused_computation.6 | convolution fusion | flops 11010048 | bytes 2228608 | tf_op jit(solution)/shard_map/shk,shkv->shv/dot_general | solution.py:384
  57.4 0.1 copy.63
  57.5 0.1 copy.64
  57.6 0.1 fusion.19
  57.6 2.9 %multiply_add_fusion = f32[8,4,128,128]{3,2,1,0:T(8,128)S(1)} fusion(f32[8,4,128]{2,1,0:T(4,128)S(1)} %fusion.19, f32[8,4,128]{2,1,0:T(4,128)S(1)} %get-tuple-element.13, f32[8,4]{1,0:T(8,128)S(1)} %copy.63, f32[8,4,128]{2,1,0:T(4,128)S(1)} %fusion.21, f32[8,4,128]{2,1,0:T(4,128)S(1)} %get-tuple-element.16, f32[8,4]{1,0:T(8,128)S(1)} %copy.60, ...), kind=kLoop, calls=%fused_computation | loop fusion | flops 6291456 | bytes 4325888 | tf_op jit(solution)/shard_map/add | solution.py:386
  60.5 0.0 copy-start.2
  60.5 0.0 copy-start.3
  60.5 1.9 %fusion.45 = f32[8,4,1,128]{3,2,1,0:T(1,128)S(1)} fusion(f32[8,4,128,1]{2,3,1,0:T(1,128)S(1)} %bitcast.165, f32[8,4,128,128]{3,2,1,0:T(8,128)S(1)} %multiply_add_fusion), kind=kOutput, calls=%fused_computation.97 | convolution fusion | flops 6291456 | bytes 2129920 | tf_op jit(solution)/shard_map/shk,shkv->shv/dot_general | solution.py:387
  62.4 0.1 multiply_bitcast_fusion
  62.5 0.1 multiply_reduce_fusion
  62.6 0.1 broadcast_multiply_fusion
  62.8 0.0 copy-done
  62.8 1.6 %fusion.17.mixed_ref = bf16[32,512]{1,0:T(8,128)(2,1)} fusion(f32[4,8,4,128]{3,2,1,0:T(4,128)S(1)} %bitcast.155, f32[32,2048]{1,0:T(8,128)} %get-tuple-element.4, f32[512]{0:T(512)S(1)} %broadcast_bitcast_fusion, f32[32]{0:T(128)S(1)} %rsqrt_reduce_fusion), kind=kLoop, calls=%fused_computation.25 | loop fusion | flops 131072 | bytes 166016 | tf_op jit(solution)/shard_map/convert_element_type | solution.py:478
  64.3 0.0 copy-done.3
  64.3 0.6 reshape.337
  64.9 88.5 %shard_map.177 = bf16[64,512]{1,0:T(8,128)(2,1)} custom-call(bf16[32,512]{1,0:T(8,128)(2,1)} %fusion.17.mixed_ref, bf16[64,512]{1,0:T(8,128)(2,1)} %x_ref.3, f32[8,1,512]{2,1,0:T(1,128)} %bitcast.162, bf16[512,512]{1,0:T(8,128)(2,1)} %w_out_hbm.1, bf16[512,2816]{1,0:T(8,128)(2,1)} %w_gate_hbm.1, bf16[512,2816]{1,0:T(8,128)(2,1)} %w_up_hbm.1, ...), custom_call_target="tpu_custom_call" | custom-call | tf_op jit(solution)/shard_map/pallas_call | solution.py:484
  153.4 0.0 copy-done.2
  153.4 1.5 copy.87
  (15 shorter events, 0.2 us)
Async XLA Ops:
  0.6 62.1 %copy-start = (f32[128]{0:T(128)S(1)}, f32[128]{0:T(128)}, u32[]{:S(2)}) copy-start(f32[128]{0:T(128)} %param.28) | copy-start | bytes 1540
  0.6 34.2 %copy-start.5 = (f32[4]{0:T(128)S(1)}, f32[4]{0:T(128)}, u32[]{:S(2)}) copy-start(f32[4]{0:T(128)} %param.27) | copy-start | bytes 52
  0.7 34.4 %copy-start.4 = (s32[8]{0:T(128)S(1)}, s32[8]{0:T(128)}, u32[]{:S(2)}) copy-start(s32[8]{0:T(128)} %param.18) | copy-start | bytes 100
  0.7 35.9 %copy-start.1 = (f32[8,4,128,128]{3,2,1,0:T(8,128)S(1)}, f32[8,4,128,128]{3,2,1,0:T(8,128)}, u32[]{:S(2)}) copy-start(f32[8,4,128,128]{3,2,1,0:T(8,128)} %param.19) | copy-start | bytes 6291460
  60.5 92.9 %copy-start.2 = (f32[8,4,128,128]{3,2,1,0:T(8,128)}, f32[8,4,128,128]{3,2,1,0:T(8,128)S(1)}, u32[]{:S(2)}) copy-start(f32[8,4,128,128]{3,2,1,0:T(8,128)S(1)} %multiply_add_fusion) | copy-start | bytes 6291460
  60.5 3.8 %copy-start.3 = (bf16[4096]{0:T(1024)(128)(2,1)S(1)}, bf16[4096]{0:T(1024)(128)(2,1)}, u32[]{:S(2)}) copy-start(bf16[4096]{0:T(1024)(128)(2,1)} %param.30) | copy-start | bytes 24580

commit v2 on v1

--- a/solution.py
+++ b/solution.py
@@ -160,82 +160,60 @@
     return total
 
 
-def project_kernel(
+def split(value):
+    high = value.astype(BF16).astype(F32)
+    return high, value - high
+
+
+def unit_norm(vectors):
+    return vectors * lax.rsqrt(jnp.sum(vectors * vectors, axis=-1, keepdims=True) + EPS)
+
+
+def softplus(value):
+    return jnp.maximum(value, 0.0) + jnp.log1p(jnp.exp(-jnp.abs(value)))
+
+
+def layer_kernel(
     n_kv,
     n_tp,
+    n_groups,
     x_ref,
-    gain_ref,
+    attn_gain_ref,
     rate_ref,
+    lengths_ref,
+    forget_ref,
+    head_gain_ref,
+    mixer_gain_ref,
     wq_hbm,
     wk_hbm,
     wv_hbm,
     wo_hbm,
-    out_ref,
-    aux_out_ref,
-    weights,
-    x_all,
-    aux,
-    aux_got,
-    parts,
-    x_got,
-    folded,
-    z_got,
-    load_sem,
-    send_sem,
-    recv_sem,
-):
-    net = Net(n_kv, n_tp, send_sem, recv_sem)
-    loads = []
-    for i, source in enumerate((wq_hbm, wk_hbm, wv_hbm, wo_hbm)):
-        copy = pltpu.make_async_copy(source, weights.at[i], load_sem.at[i])
-        copy.start()
-        loads.append(copy)
-    net.barrier()
-    incoming = gather_tp(net, x_ref, x_all)
-    x_all[net.tp] = x_ref[...]
-    arrive(incoming)
-    wide = x_all[...].reshape(-1, x_ref.shape[1]).astype(F32)
-    squares = jnp.sum(wide * wide, axis=1, keepdims=True)
-    normed = (wide * gain_ref[net.kv]).astype(BF16)
-    rates = jnp.dot(normed, rate_ref[...], preferred_element_type=F32)
-    lane = lax.broadcasted_iota(jnp.int32, rates.shape, 1)
-    aux[...] = jnp.where(lane == LANES - 1, squares, rates).reshape(aux.shape)
-    aux_in = scatter_kv(net, aux, aux_got)
-    width = weights.shape[2]
-    crossing = []
-    for i in range(4):
-        cols = pl.ds(i * width, width)
-        loads[i].wait()
-        product = jnp.dot(normed, weights[i], preferred_element_type=F32)
-        store_parts(net, parts, product, cols)
-        crossing.append(scatter_x(net, parts, x_got, cols))
-    climbing = []
-    for i in range(4):
-        cols = pl.ds(i * width, width)
-        arrive(crossing[i])
-        fold_x(net, parts, x_got, folded, cols)
-        climbing.append(scatter_z(net, folded, z_got, cols))
-    arrive(aux_in)
-    aux_out_ref[...] = aux[net.kv] + jnp.sum(aux_got[...], axis=0)
-    for i in range(4):
-        cols = pl.ds(i * width, width)
-        arrive(climbing[i])
-        out_ref[:, cols] = fold_z(net, folded, z_got, cols)
-    net.drain()
-
-
-def mixer_kernel(
-    n_kv,
-    n_tp,
-    n_groups,
-    mixed_ref,
-    x_ref,
-    gain_ref,
     w_out_hbm,
     w_gate_hbm,
     w_up_hbm,
     w_down_hbm,
+    state_hbm,
     out_ref,
+    state_out,
+    aux1,
+    aux1_got,
+    parts1,
+    x1_got,
+    folded1,
+    z1_got,
+    weights,
+    x_all,
+    state,
+    state_hi,
+    state_lo,
+    pre,
+    aux_sum,
+    lhs,
+    recalled,
+    left,
+    right,
+    keep_all,
+    mixed_rows,
     w_out,
     w_gate,
     w_up,
@@ -259,18 +237,152 @@
 ):
     net = Net(n_kv, n_tp, send_sem, recv_sem)
     loads = []
-    pairs = ((w_out_hbm, w_out), (w_gate_hbm, w_gate), (w_up_hbm, w_up), (w_down_hbm, w_down))
-    for i, (source, target) in enumerate(pairs):
-        copy = pltpu.make_async_copy(source, target, load_sem.at[i])
-        copy.start()
-        loads.append(copy)
+    pairs = (
+        (wq_hbm, weights.at[0]),
+        (wk_hbm, weights.at[1]),
+        (wv_hbm, weights.at[2]),
+        (wo_hbm, weights.at[3]),
+        (w_out_hbm, w_out),
+        (w_gate_hbm, w_gate),
+        (w_up_hbm, w_up),
+        (w_down_hbm, w_down),
+        (state_hbm, state),
+    )
+    for i in (0, 1, 2, 3, 8, 4, 5, 6, 7):
+        pltpu.make_async_copy(*pairs[i], load_sem.at[i]).start()
+    loads = [pltpu.make_async_copy(*pair, load_sem.at[i]) for i, pair in enumerate(pairs)]
     net.barrier()
-    incoming = gather_kv(net, mixed_ref, mixed_all)
-    mixed_all[net.kv] = mixed_ref[...]
+    incoming = gather_tp(net, x_ref, x_all)
+    x_all[net.tp] = x_ref[...]
     arrive(incoming)
-    loads[0].wait()
+    wide = x_all[...].reshape(-1, x_ref.shape[1]).astype(F32)
+    squares = jnp.sum(wide * wide, axis=1, keepdims=True)
+    normed = (wide * attn_gain_ref[net.kv]).astype(BF16)
+    rates = jnp.dot(normed, rate_ref[...], preferred_element_type=F32)
+    lane = lax.broadcasted_iota(jnp.int32, rates.shape, 1)
+    aux1[...] = jnp.where(lane == LANES - 1, squares, rates).reshape(aux1.shape)
+    aux_in = scatter_kv(net, aux1, aux1_got)
+    width = weights.shape[2]
+    crossing = []
+    for i in range(4):
+        cols = pl.ds(i * width, width)
+        loads[i].wait()
+        product = jnp.dot(normed, weights[i], preferred_element_type=F32)
+        store_parts(net, parts1, product, cols)
+        crossing.append(scatter_x(net, parts1, x1_got, cols))
+    climbing = []
+    for i in range(4):
+        cols = pl.ds(i * width, width)
+        arrive(crossing[i])
+        fold_x(net, parts1, x1_got, folded1, cols)
+        climbing.append(scatter_z(net, folded1, z1_got, cols))
+
+    seqs, heads, size = state.shape[0], state.shape[1], state.shape[2]
+    pieces = seqs * heads
+    arrive(aux_in)
+    aux_sum[...] = aux1[net.kv] + jnp.sum(aux1_got[...], axis=0)
+    loads[8].wait()
+    for h in range(heads):
+        for s in range(seqs):
+            high = state[s, h].astype(BF16)
+            state_hi[h * seqs + s] = high
+            state_lo[h * seqs + s] = (state[s, h] - high.astype(F32)).astype(BF16)
+    for i in range(4):
+        cols = pl.ds(i * width, width)
+        arrive(climbing[i])
+        total = fold_z(net, folded1, z1_got, cols)
+        for h in range(heads):
+            pre[i * heads + h] = total[:, h * size : (h + 1) * size]
+
+    def stacked(at, t):
+        return jnp.concatenate(
+            [
+                pre[at * heads + h, pl.ds(t, seqs, stride=NEW), :]
+                for h in range(heads)
+            ],
+            axis=0,
+        )
+
+    def tall(parts_of):
+        return jnp.concatenate(parts_of, axis=0)
+
+    keys, values, queries, writes, keeps, lives, scales = [], [], [], [], [], [], []
+    for t in range(NEW):
+        sums = aux_sum[pl.ds(t, seqs, stride=NEW), :]
+        row_scale = lax.rsqrt(sums[:, LANES - 1 :] / D + EPS)
+        live_rows = (lengths_ref[...] > t).astype(F32)
+        scale = tall([row_scale] * heads)
+        live = tall([live_rows] * heads)
+        write = tall([sums[:, h : h + 1] for h in range(heads)]) * scale
+        forget = tall([sums[:, heads + h : heads + h + 1] for h in range(heads)]) * scale
+        rate = tall([jnp.full((seqs, 1), forget_ref[h], F32) for h in range(heads)])
+        scales.append(scale)
+        lives.append(live)
+        writes.append(jax.nn.sigmoid(write) * live)
+        keeps.append(jnp.exp(-rate * softplus(forget) * live))
+        queries.append(unit_norm(jax.nn.silu(stacked(0, t) * scale)) * size ** (-0.5))
+        keys.append(unit_norm(jax.nn.silu(stacked(1, t) * scale)))
+        values.append(jax.nn.silu(stacked(2, t) * scale))
+        k_high, k_low = split(keys[t])
+        q_high, q_low = split(queries[t])
+        for place, rows in enumerate((k_high, q_high, k_low, q_low)):
+            lhs[pl.ds(place * NEW + t, pieces, stride=4 * NEW), :] = rows
+    for i in range(pieces):
+        block = lhs[i * 4 * NEW : (i + 1) * 4 * NEW, :].astype(BF16)
+        product = jnp.dot(block, state_hi[i], preferred_element_type=F32)
+        product = product + jnp.dot(block, state_lo[i], preferred_element_type=F32)
+        recalled[i * 2 * NEW : (i + 1) * 2 * NEW, :] = product[: 2 * NEW] + product[2 * NEW :]
+    ahead = jnp.ones((pieces, 1), F32)
+    decay, updates = [], []
+    for t in range(NEW):
+        seen = ahead * recalled[pl.ds(t, pieces, stride=2 * NEW), :]
+        for j in range(t):
+            match = jnp.sum(keys[t] * keys[j], axis=-1, keepdims=True)
+            seen = seen + (decay[j] * match) * updates[j]
+        updates.append(writes[t] * (values[t] - keeps[t] * seen))
+        ahead = ahead * keeps[t]
+        decay = [item * keeps[t] for item in decay] + [jnp.ones((pieces, 1), F32)]
+        reading = ahead * recalled[pl.ds(NEW + t, pieces, stride=2 * NEW), :]
+        for j in range(t + 1):
+            match = jnp.sum(queries[t] * keys[j], axis=-1, keepdims=True)
+            reading = reading + (decay[j] * match) * updates[j]
+        reading = reading * lives[t]
+        normed_out = reading * lax.rsqrt(jnp.mean(reading * reading, axis=-1, keepdims=True) + EPS)
+        normed_out = normed_out * head_gain_ref[...] * jax.nn.silu(stacked(3, t) * scales[t])
+        for h in range(heads):
+            mixed_rows[h, pl.ds(t, seqs, stride=NEW), :] = normed_out[h * seqs : (h + 1) * seqs]
+
+    def update_state():
+        keep_all[...] = jnp.broadcast_to(ahead, keep_all.shape)
+        for j in range(NEW):
+            k_high, k_low = split(decay[j] * keys[j])
+            u_high, u_low = split(updates[j])
+            for place, rows in enumerate((k_high, k_low, k_high, k_low)):
+                left[pl.ds(place * NEW + j, pieces, stride=4 * NEW), :] = rows
+            for place, rows in enumerate((u_high, u_high, u_low, u_low)):
+                right[pl.ds(place * NEW + j, pieces, stride=4 * NEW), :] = rows
+        for h in range(heads):
+            for s in range(seqs):
+                i = h * seqs + s
+                rows = slice(i * 4 * NEW, (i + 1) * 4 * NEW)
+                gained = lax.dot_general(
+                    left[rows, :].astype(BF16),
+                    right[rows, :].astype(BF16),
+                    (((0,), (0,)), ((), ())),
+                    preferred_element_type=F32,
+                )
+                state[s, h] = keep_all[i : i + 1, :] * state[s, h] + gained
+
+    for h in range(heads):
+        mixed_all[net.kv, :, pl.ds(h * size, size)] = mixed_rows[h].astype(BF16)
+    incoming = gather_kv(net, mixed_all.at[net.kv], mixed_all)
+    update_state()
+    saving = pltpu.make_async_copy(state, state_out, load_sem.at[9])
+    saving.start()
+    arrive(incoming)
+    loads[0 + 4].wait()
     terms = jnp.dot(
-        mixed_all[...].reshape(-1, mixed_ref.shape[1]), w_out[...], preferred_element_type=F32
+        mixed_all[...].reshape(-1, width), w_out[...], preferred_element_type=F32
     )
     out_parts[...] = terms.astype(BF16).reshape(out_parts.shape)
     arrive(scatter_tp(net, out_parts, out_got))
@@ -282,14 +394,14 @@
     arrive(gather_tp(net, hidden_all.at[net.tp], hidden_all))
     wide = hidden_all[...].reshape(-1, x_ref.shape[1]).astype(F32)
     squares = jnp.sum(wide * wide, axis=1, keepdims=True)
-    normed = (wide * gain_ref[net.kv]).astype(BF16)
+    normed = (wide * mixer_gain_ref[net.kv]).astype(BF16)
     aux[...] = jnp.broadcast_to(squares, (squares.shape[0], LANES)).reshape(aux.shape)
     aux_in = scatter_kv(net, aux, aux_got)
     spans = groups_of(w_gate.shape[1], n_groups)
     count = len(spans)
     crossing, climbing, rising, spreading = [], [], [], []
-    loads[1].wait()
-    loads[2].wait()
+    loads[1 + 4].wait()
+    loads[2 + 4].wait()
     for at, size in spans:
         store_parts(
             net,
@@ -309,7 +421,7 @@
     for d in range(1, n_kv):
         total = total + aux_got[d - 1]
     scale = lax.rsqrt(total[:, :1] / D + EPS)
-    loads[3].wait()
+    loads[3 + 4].wait()
     down = None
     for step in range(count + 3):
         if step < count:
@@ -353,6 +465,7 @@
     for d in range(1, n_tp):
         result = result + down_got[d - 1].astype(F32)
     out_ref[...] = (hidden_all[net.tp].astype(F32) + result).astype(BF16)
+    saving.wait()
     net.drain()
 
 
@@ -368,27 +481,6 @@
     return pltpu.CompilerParams(
         collective_id=collective_id, has_side_effects=True, vmem_limit_bytes=56 * 1024 * 1024
     )
-
-
-def unit_norm(vectors):
-    return vectors * lax.rsqrt(jnp.sum(vectors * vectors, axis=-1, keepdims=True) + EPS)
-
-
-def run_delta(carried, query_unit, key_unit, value_act, write_rate, log_keep, live):
-    readings = []
-    for position in range(query_unit.shape[1]):
-        active = live[:, position][:, None]
-        beta = write_rate[:, position] * active
-        keep = jnp.exp(log_keep[:, position] * active)
-        key_now = key_unit[:, position]
-        recalled = jnp.einsum("shk,shkv->shv", key_now, carried, precision=lax.Precision.HIGHEST)
-        update = beta[:, :, None] * (value_act[:, position] - keep[:, :, None] * recalled)
-        carried = keep[:, :, None, None] * carried + key_now[:, :, :, None] * update[:, :, None, :]
-        reading = jnp.einsum(
-            "shk,shkv->shv", query_unit[:, position], carried, precision=lax.Precision.HIGHEST
-        )
-        readings.append(reading * active[:, :, None])
-    return (carried, jnp.stack(readings, axis=1))
 
 
 def local(
@@ -417,31 +509,67 @@
     own = rows // n_kv
     nz, nx = grid_of(n_kv)
     head_cols = w_query.shape[1]
-    seqs_here = seq_lengths.shape[0]
-    heads_here = forget_rate.shape[0]
-    head_size = head_gain.shape[0]
+    seqs, heads, size = delta_state.shape[:3]
+    pieces = seqs * heads
+    hidden_cols = w_gate.shape[1]
     rate_weight = jnp.pad(
-        jnp.concatenate([w_write, w_forget], axis=1), ((0, 0), (0, LANES - 2 * heads_here))
+        jnp.concatenate([w_write, w_forget], axis=1), ((0, 0), (0, LANES - 2 * heads))
     )
-    copies = (n_tp - 1) + (n_kv - 1) + 4 * (nx - 1 + nz - 1)
-    sums, aux = pl.pallas_call(
-        functools.partial(project_kernel, n_kv, n_tp),
-        out_shape=(
-            jax.ShapeDtypeStruct((own, 4 * head_cols), F32),
-            jax.ShapeDtypeStruct((own, LANES), F32),
-        ),
-        in_specs=[vmem()] * 3 + [hbm()] * 4,
-        out_specs=(vmem(), vmem()),
-        scratch_shapes=[
-            pltpu.VMEM((4, features, head_cols), BF16),
-            pltpu.VMEM((n_tp, tp_rows, features), BF16),
+    n_groups = 6
+    groups = len(groups_of(hidden_cols, n_groups))
+    copies = 4 * (n_tp - 1) + 3 * (n_kv - 1) + (2 * groups + 4) * (nx - 1 + nz - 1)
+
+    def reduce_buffers(cols):
+        return [
             pltpu.VMEM((n_kv, own, LANES), F32),
             pltpu.VMEM((n_kv - 1, own, LANES), F32),
-            pltpu.VMEM((nx, nz * own, 4 * head_cols), BF16),
-            pltpu.VMEM((nx - 1, nz * own, 4 * head_cols), BF16),
-            pltpu.VMEM((nz, own, 4 * head_cols), BF16),
-            pltpu.VMEM((nz - 1, own, 4 * head_cols), BF16),
-            pltpu.SemaphoreType.DMA((4,)),
+            pltpu.VMEM((nx, nz * own, cols), BF16),
+            pltpu.VMEM((nx - 1, nz * own, cols), BF16),
+            pltpu.VMEM((nz, own, cols), BF16),
+            pltpu.VMEM((nz - 1, own, cols), BF16),
+        ]
+
+    row_block = pltpu.VMEM((n_tp, tp_rows, features), BF16)
+    row_got = pltpu.VMEM((n_tp - 1, tp_rows, features), BF16)
+    smem = pl.BlockSpec(memory_space=pltpu.SMEM)
+    return pl.pallas_call(
+        functools.partial(layer_kernel, n_kv, n_tp, n_groups),
+        out_shape=(
+            jax.ShapeDtypeStruct((tp_rows, features), BF16),
+            jax.ShapeDtypeStruct(delta_state.shape, F32),
+        ),
+        in_specs=[vmem()] * 4 + [smem] + [vmem()] * 2 + [hbm()] * 9,
+        out_specs=(vmem(), hbm()),
+        scratch_shapes=reduce_buffers(4 * head_cols)
+        + [
+            pltpu.VMEM((4, features, head_cols), BF16),
+            row_block,
+            pltpu.VMEM(delta_state.shape, F32),
+            pltpu.VMEM((pieces, size, size), BF16),
+            pltpu.VMEM((pieces, size, size), BF16),
+            pltpu.VMEM((4 * heads, own, size), F32),
+            pltpu.VMEM((own, LANES), F32),
+            pltpu.VMEM((pieces * 4 * NEW, size), F32),
+            pltpu.VMEM((pieces * 2 * NEW, size), F32),
+            pltpu.VMEM((pieces * 4 * NEW, size), F32),
+            pltpu.VMEM((pieces * 4 * NEW, size), F32),
+            pltpu.VMEM((pieces, LANES), F32),
+            pltpu.VMEM((heads, own, size), F32),
+            pltpu.VMEM(w_out.shape, BF16),
+            pltpu.VMEM(w_gate.shape, BF16),
+            pltpu.VMEM(w_up.shape, BF16),
+            pltpu.VMEM(w_down.shape, BF16),
+            pltpu.VMEM((n_kv, own, head_cols), BF16),
+            row_block,
+            row_got,
+            row_block,
+        ]
+        + reduce_buffers(2 * hidden_cols)
+        + [
+            pltpu.VMEM((nz, nx, own, hidden_cols), BF16),
+            row_block,
+            row_got,
+            pltpu.SemaphoreType.DMA((10,)),
             pltpu.SemaphoreType.DMA((copies,)),
             pltpu.SemaphoreType.DMA((copies,)),
         ],
@@ -450,75 +578,20 @@
         layer_input,
         attn_gain.astype(F32).reshape(n_kv, 1, features),
         rate_weight,
+        seq_lengths.reshape(seqs, 1),
+        forget_rate,
+        head_gain.reshape(1, size),
+        mixer_gain.astype(F32).reshape(n_kv, 1, features),
         w_query,
         w_key,
         w_value,
         w_outgate,
-    )
-    row_scale = lax.rsqrt(aux[:, LANES - 1 :] / D + EPS)
-
-    def split_heads(at):
-        block = sums[:, at * head_cols : (at + 1) * head_cols]
-        return (block * row_scale).reshape(seqs_here, NEW, heads_here, head_size)
-
-    query_unit = unit_norm(jax.nn.silu(split_heads(0))) * head_size ** (-0.5)
-    key_unit = unit_norm(jax.nn.silu(split_heads(1)))
-    value_act = jax.nn.silu(split_heads(2))
-    outgate = split_heads(3)
-    rate_rows = (aux[:, : 2 * heads_here] * row_scale).reshape(seqs_here, NEW, 2 * heads_here)
-    write_rate = jax.nn.sigmoid(rate_rows[:, :, :heads_here])
-    log_keep = -forget_rate * jax.nn.softplus(rate_rows[:, :, heads_here:])
-    positions = jnp.arange(NEW, dtype=jnp.int32)
-    live = (positions[None, :] < seq_lengths[:, None]).astype(F32)
-    carried, readings = run_delta(
-        delta_state, query_unit, key_unit, value_act, write_rate, log_keep, live
-    )
-    normed = readings * lax.rsqrt(jnp.mean(readings * readings, axis=-1, keepdims=True) + EPS)
-    normed = normed * head_gain * jax.nn.silu(outgate)
-    mixed = normed.reshape(own, heads_here * head_size).astype(BF16)
-
-    hidden_cols = w_gate.shape[1]
-    n_groups = 6
-    groups = len(groups_of(hidden_cols, n_groups))
-    copies = 3 * (n_tp - 1) + 2 * (n_kv - 1) + 2 * groups * (nx - 1 + nz - 1)
-    layer_output = pl.pallas_call(
-        functools.partial(mixer_kernel, n_kv, n_tp, n_groups),
-        out_shape=jax.ShapeDtypeStruct((tp_rows, features), BF16),
-        in_specs=[vmem()] * 3 + [hbm()] * 4,
-        out_specs=vmem(),
-        scratch_shapes=[
-            pltpu.VMEM(w_out.shape, BF16),
-            pltpu.VMEM(w_gate.shape, BF16),
-            pltpu.VMEM(w_up.shape, BF16),
-            pltpu.VMEM(w_down.shape, BF16),
-            pltpu.VMEM((n_kv, own, head_cols), BF16),
-            pltpu.VMEM((n_tp, tp_rows, features), BF16),
-            pltpu.VMEM((n_tp - 1, tp_rows, features), BF16),
-            pltpu.VMEM((n_tp, tp_rows, features), BF16),
-            pltpu.VMEM((n_kv, own, LANES), F32),
-            pltpu.VMEM((n_kv - 1, own, LANES), F32),
-            pltpu.VMEM((nx, nz * own, 2 * hidden_cols), BF16),
-            pltpu.VMEM((nx - 1, nz * own, 2 * hidden_cols), BF16),
-            pltpu.VMEM((nz, own, 2 * hidden_cols), BF16),
-            pltpu.VMEM((nz - 1, own, 2 * hidden_cols), BF16),
-            pltpu.VMEM((nz, nx, own, hidden_cols), BF16),
-            pltpu.VMEM((n_tp, tp_rows, features), BF16),
-            pltpu.VMEM((n_tp - 1, tp_rows, features), BF16),
-            pltpu.SemaphoreType.DMA((4,)),
-            pltpu.SemaphoreType.DMA((copies,)),
-            pltpu.SemaphoreType.DMA((copies,)),
-        ],
-        compiler_params=params(1),
-    )(
-        mixed,
-        layer_input,
-        mixer_gain.astype(F32).reshape(n_kv, 1, features),
         w_out,
         w_gate,
         w_up,
         w_down,
+        delta_state,
     )
-    return (layer_output, carried)
 
 
 def solution(mesh):

time: 155 us -> 125 us (0.81)
  matrix products: 21.6 us -> 0 us
  other arithmetic: 11.3 us -> 3.31 us
  Pallas kernels: 118 us -> 114 us
  local copies, waits for them, and re-layouts: 3.4 us -> 6.78 us
    dot_general x8 -> x0, matrix products: 21.6 us -> none  [the longest x4 10.9 us: run_delta(): jnp.einsum('shk,shkv->shv', query_unit[:, position], carried, precision=l...]
    pallas_call x2 -> x1, Pallas kernels: 118 us -> 114 us  [local(): pl.pallas_call(functools.partial(layer_kernel, n_kv, n_tp, n_groups), out...]
    unnamed x15 -> x2, local copies, waits for them, and re-layouts: 1.72 us -> 4.61 us
    add x1 -> x0, other arithmetic: 2.85 us -> none  [run_delta(): keep[:, :, None, None] * carried]
    mul x11 -> x0, other arithmetic: 2.55 us -> none  [the longest x1 0.99 us: split_heads(): return (block * row_scale).reshape(seqs_here, NEW, heads_here, head_size)]
    convert_element_type x2 -> x0, other arithmetic: 1.56 us -> none  [the longest x1 1.56 us: local(): mixed = normed.reshape(own, heads_here * head_size).astype(BF16)]
where the time goes in v2:
time: 125 us
  Pallas kernels  114 us (91%)
  local copies, waits for them, and re-layouts  6.78 us (5%)
  other arithmetic  3.31 us (3%)
    pallas_call x1, Pallas kernels, local(): pl.pallas_call(functools.partial(layer_kernel, n_kv, n_tp, n_groups), out...  114 us
    unnamed x2, local copies, waits for them, and re-layouts  4.61 us

profile of v2, /device:TPU:1, one launch (start us, length us, event | category | flops | bytes accessed | tf_op | source)
XLA Modules:
  0.0 125.1 jit_solution(1540579367686467888)
XLA Ops:
  0.6 1.3 %copy.23.lengths_ref = s32[8,1]{1,0:T(8,128)} copy(s32[8,1]{0,1:T(1,128)} %bitcast.7) | data formatting | bytes 64 | tf_op jit(solution)/shard_map/reshape | solution.py:581
  2.0 0.7 pad_maximum_fusion
  2.7 1.3 %reshape.26 = f32[4096]{0:T(1024)} convert(bf16[4096]{0:T(1024)(128)(2,1)} %param.20) | non-fusion elementwise | flops 4096 | bytes 24576 | tf_op jit(solution)/shard_map/reshape | solution.py:579
  4.0 1.3 %reshape.28 = f32[4096]{0:T(1024)} convert(bf16[4096]{0:T(1024)(128)(2,1)} %param.30) | non-fusion elementwise | flops 4096 | bytes 24576 | tf_op jit(solution)/shard_map/reshape | solution.py:584
  5.3 0.2 copy.22
  5.4 0.7 pad.4.rate_ref
  6.1 114.3 %shard_map.176 = (bf16[64,512]{1,0:T(8,128)(2,1)}, f32[8,4,128,128]{3,2,1,0:T(8,128)}) custom-call(bf16[64,512]{1,0:T(8,128)(2,1)} %x_ref.1, f32[8,1,512]{2,1,0:T(1,128)} %bitcast.4, bf16[512,128]{1,0:T(8,128)(2,1)} %pad.4.rate_ref, s32[8,1]{1,0:T(8,128)} %copy.23.lengths_ref, f32[4]{0:T(128)} %forget_ref.1, f32[1,128]{1,0:T(1,128)} %bitcast.6, ...), custom_call_target="tpu_custom_call" | custom-call | tf_op jit(solution)/shard_map/pallas_call | solution.py:535
  120.5 1.5 %copy.26 = bf16[64,512]{1,0:T(8,128)(2,1)} copy(bf16[64,512]{1,0:T(8,128)(2,1)} %get-tuple-element.4) | data formatting | bytes 131072
  121.9 3.1 %copy.27 = f32[8,4,128,128]{3,2,1,0:T(8,128)} copy(f32[8,4,128,128]{3,2,1,0:T(8,128)} %get-tuple-element.5) | data formatting | bytes 4194304
